TPU v7x, 32 devices: a whole 2x2x4 slice. The times are simulated.
32 devices in a mesh: tp: 8 (over z, y), dp: 4 (over x, core).
Axes of the slice: x: 2, y: 2, z: 4, core: 2. Of those that a mesh axis runs over, the one named last changes fastest.
Arguments:
- activation_rows: bfloat16 [1024, 4096], P(None, 'dp'), may hold values from -24 to 24
- fresh_spans: int32 [128], P('dp'), may hold values from 1 to 8, 384 in all
- entry_rescale_vector: float32 [2, 4096], P(None, 'dp'), may hold values from 0.1 to 1.9
- probe_kernel: bfloat16 [2, 4096, 4096], P(None, 'dp', 'tp'), may hold values from -0.09375 to 0.09375
- retention_kernel: bfloat16 [2, 4096, 4096], P(None, 'dp', 'tp'), may hold values from -0.09375 to 0.09375
- content_kernel: bfloat16 [2, 4096, 4096], P(None, 'dp', 'tp'), may hold values from -0.09375 to 0.09375
- valve_kernel: bfloat16 [2, 4096, 4096], P(None, 'dp', 'tp'), may hold values from -0.09375 to 0.09375
- retention_minimum: float32 [2, 4096], P(None, 'tp'), may hold values from 0 to 0.99
- extra_attenuation: float32 [2, 1024, 32], P(None, 'dp', 'tp'), may hold values from -0.7 to 0
- channel_rescale_vector: float32 [2, 4096], P(None, 'tp'), may hold values from 0.1 to 1.9
- emission_kernel: bfloat16 [2, 4096, 4096], P(None, 'tp', 'dp'), may hold values from -0.09375 to 0.09375
- memory_grids: float32 [2, 128, 32, 128, 128], P(None, 'dp', 'tp'), may hold values from -0.6 to 0.6
Outputs:
- mixed: bfloat16 [1024, 4096], P(None, 'dp')
- new_states: float32 [2, 128, 32, 128, 128], P(None, 'dp', 'tp')
Inputs may be any that keep to these rules, and one draw needn't show every extreme that they name: `fresh_spans`: each sequence has at least one live slot.
All inputs are finite; a program needn't handle non-finite values. No bound on the sum of `fresh_spans` on one device may be relied on, other than what follows from the above.
Results may differ from a plain program's by a relative error of at most 0.017.
Values may be sent and summed in bfloat16 or wider, within the bound.
A program may use at most 128 MiB of HBM per device.

v0:
```python
import jax
import jax.numpy as jnp
from jax import lax
from jax.sharding import PartitionSpec as P

D = 4096
BLOCKS = 2


EPSILON = 1e-05


def update_tick(
    probe_scores,
    retention_scores,
    content_scores,
    valve_scores,
    minimum_bound,
    spike_ledger,
    attention_multiplier,
    stream_spans,
    memory_grid,
):
    stream_tally = memory_grid.shape[0]
    attention_tally = memory_grid.shape[1]
    key_dim = memory_grid.shape[2]
    value_dim = memory_grid.shape[3]
    position_tally = probe_scores.shape[0] // stream_tally

    def split_heads(array, width):
        return array.astype(jnp.float32).reshape(
            stream_tally, position_tally, attention_tally, width
        )

    queries = jax.nn.silu(split_heads(probe_scores, key_dim))
    forget_in = split_heads(retention_scores, key_dim)
    lower_heads = minimum_bound.reshape(attention_tally, key_dim)
    retention_sigmoid = lower_heads + (1.0 - lower_heads) * jax.nn.sigmoid(forget_in)
    key_vecs = (1.0 - lower_heads) * jax.nn.sigmoid(-forget_in)
    log_attenuation = (
        jnp.log(retention_sigmoid)
        + spike_ledger.reshape(stream_tally, position_tally, attention_tally)[..., None]
    )
    values = split_heads(content_scores, value_dim)
    positions = lax.broadcasted_iota(jnp.int32, (stream_tally, position_tally), 1)
    live_mask = positions < stream_spans[:, None]

    def advance(matrix, inputs):
        query_now, key_now, decay_now, value_now, live_now = inputs
        updated = (
            jnp.exp(decay_now)[..., None] * matrix + key_now[..., None] * value_now[..., None, :]
        )
        matrix = jnp.where(live_now[:, None, None, None], updated, matrix)
        readout = jnp.einsum("shkv,shk->shv", matrix, query_now, precision=lax.Precision.HIGHEST)
        return (matrix, readout)

    ending_emission, readouts = lax.scan(
        advance,
        memory_grid,
        (
            jnp.moveaxis(queries, 1, 0),
            jnp.moveaxis(key_vecs, 1, 0),
            jnp.moveaxis(log_attenuation, 1, 0),
            jnp.moveaxis(values, 1, 0),
            jnp.moveaxis(live_mask, 1, 0),
        ),
    )
    readouts = jnp.moveaxis(readouts, 0, 1)
    normed = readouts * lax.rsqrt(jnp.mean(readouts * readouts, axis=-1, keepdims=True) + EPSILON)
    normed = (
        normed
        * attention_multiplier.reshape(attention_tally, value_dim)
        * jax.nn.silu(split_heads(valve_scores, value_dim))
    )
    normed = normed * live_mask.astype(jnp.float32)[..., None, None]
    return (
        normed.reshape(stream_tally * position_tally, attention_tally * value_dim).astype(
            jnp.bfloat16
        ),
        ending_emission,
    )


def local(
    activation_rows,
    fresh_spans,
    entry_rescale_vector,
    probe_kernel,
    retention_kernel,
    content_kernel,
    valve_kernel,
    retention_minimum,
    extra_attenuation,
    channel_rescale_vector,
    emission_kernel,
    memory_grids,
):
    residual = activation_rows
    own_rows = activation_rows.shape[0] // lax.axis_size("dp")
    finals = []
    for layer_index in range(BLOCKS):
        current = residual.astype(jnp.float32)
        squares = lax.psum(jnp.sum(current * current, axis=1), "dp")
        row_scale = lax.rsqrt(squares / D + EPSILON)
        normed = (current * entry_rescale_vector[layer_index]).astype(jnp.bfloat16)
        weights = (
            probe_kernel[layer_index],
            retention_kernel[layer_index],
            content_kernel[layer_index],
            valve_kernel[layer_index],
        )

        def project():
            return jnp.concatenate(
                [jnp.dot(normed, weight, preferred_element_type=jnp.float32) for weight in weights],
                axis=1,
            )

        summed = lax.psum_scatter(
            project().astype(jnp.bfloat16), "dp", scatter_dimension=0, tiled=True
        ).astype(jnp.float32)
        own_scale = lax.dynamic_slice_in_dim(
            row_scale, lax.axis_index("dp") * own_rows, own_rows, 0
        )
        scaled = (summed * own_scale[:, None]).astype(jnp.bfloat16)
        bounds = [0]
        for weight in weights:
            bounds.append(bounds[-1] + weight.shape[1])
        pieces = [scaled[:, bounds[index] : bounds[index + 1]] for index in range(4)]
        attention_yields, ending_emission = update_tick(
            pieces[0],
            pieces[1],
            pieces[2],
            pieces[3],
            retention_minimum[layer_index],
            extra_attenuation[layer_index],
            channel_rescale_vector[layer_index],
            fresh_spans,
            memory_grids[layer_index],
        )
        finals.append(ending_emission)
        out_weight = emission_kernel[layer_index]
        partial_value = jnp.dot(
            lax.all_gather(attention_yields, "dp", axis=0, tiled=True),
            out_weight,
            preferred_element_type=jnp.float32,
        )
        update = lax.psum(partial_value.astype(jnp.bfloat16), "tp")
        residual = (current + update.astype(jnp.float32)).astype(jnp.bfloat16)
    return (residual, jnp.stack(finals))


def solution(mesh):
    placed = (
        P(None, "dp"),
        P("dp"),
        P(None, "dp"),
        P(None, "dp", "tp"),
        P(None, "dp", "tp"),
        P(None, "dp", "tp"),
        P(None, "dp", "tp"),
        P(None, "tp"),
        P(None, "dp", "tp"),
        P(None, "tp"),
        P(None, "tp", "dp"),
        P(None, "dp", "tp", None, None),
    )
    return jax.shard_map(
        local,
        mesh=mesh,
        in_specs=placed,
        out_specs=(P(None, "dp"), P(None, "dp", "tp", None, None)),
        check_vma=False,
    )
```

profile of v0, /device:TPU:0, one launch (start us, length us, event | category | flops | bytes accessed | tf_op | source)
XLA Modules:
  0.0 776.6 jit_solution(9495806767793799022)
XLA Ops:
  8.1 3.5 convolution_convert_fusion.6
  16.1 2.3 pad_maximum_fusion.1
  19.7 8.4 %psum.28 = f32[1024]{0:T(1024)S(1)} all-reduce(f32[1024]{0:T(1024)S(1)} %fusion.7), channel_id=1, replica_groups=mesh['tp'=8,'dp'=4] {'dp'}, use_global_device_ids=true, to_apply=%region_2.0 | all-reduce | flops 1024 | bytes 8192 | tf_op jit(solution)/shard_map/psum | solution.py:103
  28.3 12.2 %slice_bitcast_fusion = (f32[32,4,128,128]{3,2,1,0:T(8,128)}, f32[32,4,128,128]{3,2,1,0:T(8,128)}) fusion(f32[2,32,4,128,128]{4,3,2,1,0:T(8,128)} %param.27), kind=kLoop, calls=%fused_computation.21 | loop fusion | bytes 33554432 | tf_op jit(solution)/shard_map/squeeze | solution.py:139
  40.6 25.1 %reduce-scatter.3.cloned.1.call-done = bf16[256,2048]{0,1:T(8,128)(2,1)} async-done(((bf16[1024,2048]{0,1:T(8,128)(2,1)}), bf16[256,2048]{0,1:T(8,128)(2,1)}) %reduce-scatter.3.cloned.1.call-update) | async-done | bytes 1048592 | tf_op jit(solution)/shard_map/reduce_scatter | solution.py:119
  65.7 1.4 multiply_convert_fusion.1
  70.5 183.0 %while.24 = (s32[]{:T(128)}, f32[32,4,128,128]{3,2,1,0:T(8,128)}, f32[8,32,4,128]{3,0,2,1:T(8,128)S(1)}, pred[8,32]{1,0:T(8,128)(4,1)S(1)}, f32[8,32,4,128]{3,0,...) while((s32[]{:T(128)}, f32[32,4,128,128]{3,2,1,0:T(8,128)}, ...), condition=%wide.region_4.5_spmd, body=%wide.region_3.4_spmd.sunk | while | flops 33554432 | bytes 26149088 | solution.py:57
  70.5 1.3 constant_dynamic-slice_fusion.10
  71.9 10.5 %add_select_fusion.4 = f32[32,4,128,128]{3,2,1,0:T(8,128)} fusion(f32[32,4,128,128]{3,2,1,0:T(8,128)} %get-tuple-element.320, f32[32,4,128]{2,1,0:T(4,128)S(1)} %bitcast.274, f32[32,4,128]{2,1,0:T(4,128)S(1)} %bitcast.275, f32[32,4,128]{2,1,0:T(4,128)S(1)} %exponential_bitcast_fusion.4, pred[32]{0:T(512)(128)(4,1)S(1)} %dynamic-slice_bitcast_fusion.4), kind=kLoop, calls=%fused_computation.clone.1 | loop fusion | flops 8388608 | bytes 16973856 | tf_op jit(solution)/shard_map/while/body/eval_jaxpr/jit(_where)/select_n | solution.py:53
  82.5 9.5 %convolution_bitcast_fusion.4 = f32[1,32,4,128]{3,0,2,1:T(1,128)S(1)} fusion(f32[32,4,128,128]{3,2,1,0:T(8,128)} %add_select_fusion.4, f32[8,32,4,128]{3,0,2,1:T(8,128)S(1)} %get-tuple-element.336, s32[]{:T(128)S(6)} %copy.127), kind=kOutput, calls=%fused_computation.1.clone.1 | convolution fusion | flops 25165824 | bytes 8519684 | tf_op jit(solution)/shard_map/while/body/eval_jaxpr/shkv,shk->shv/dot_general | solution.py:54
  93.4 1.3 constant_dynamic-slice_fusion.10
  94.8 10.5 %add_select_fusion.4 = f32[32,4,128,128]{3,2,1,0:T(8,128)} fusion(f32[32,4,128,128]{3,2,1,0:T(8,128)} %get-tuple-element.320, f32[32,4,128]{2,1,0:T(4,128)S(1)} %bitcast.274, f32[32,4,128]{2,1,0:T(4,128)S(1)} %bitcast.275, f32[32,4,128]{2,1,0:T(4,128)S(1)} %exponential_bitcast_fusion.4, pred[32]{0:T(512)(128)(4,1)S(1)} %dynamic-slice_bitcast_fusion.4), kind=kLoop, calls=%fused_computation.clone.1 | loop fusion | flops 8388608 | bytes 16973856 | tf_op jit(solution)/shard_map/while/body/eval_jaxpr/jit(_where)/select_n | solution.py:53
  105.4 9.5 %convolution_bitcast_fusion.4 = f32[1,32,4,128]{3,0,2,1:T(1,128)S(1)} fusion(f32[32,4,128,128]{3,2,1,0:T(8,128)} %add_select_fusion.4, f32[8,32,4,128]{3,0,2,1:T(8,128)S(1)} %get-tuple-element.336, s32[]{:T(128)S(6)} %copy.127), kind=kOutput, calls=%fused_computation.1.clone.1 | convolution fusion | flops 25165824 | bytes 8519684 | tf_op jit(solution)/shard_map/while/body/eval_jaxpr/shkv,shk->shv/dot_general | solution.py:54
  116.2 1.3 constant_dynamic-slice_fusion.10
  117.7 10.5 %add_select_fusion.4 = f32[32,4,128,128]{3,2,1,0:T(8,128)} fusion(f32[32,4,128,128]{3,2,1,0:T(8,128)} %get-tuple-element.320, f32[32,4,128]{2,1,0:T(4,128)S(1)} %bitcast.274, f32[32,4,128]{2,1,0:T(4,128)S(1)} %bitcast.275, f32[32,4,128]{2,1,0:T(4,128)S(1)} %exponential_bitcast_fusion.4, pred[32]{0:T(512)(128)(4,1)S(1)} %dynamic-slice_bitcast_fusion.4), kind=kLoop, calls=%fused_computation.clone.1 | loop fusion | flops 8388608 | bytes 16973856 | tf_op jit(solution)/shard_map/while/body/eval_jaxpr/jit(_where)/select_n | solution.py:53
  128.2 9.5 %convolution_bitcast_fusion.4 = f32[1,32,4,128]{3,0,2,1:T(1,128)S(1)} fusion(f32[32,4,128,128]{3,2,1,0:T(8,128)} %add_select_fusion.4, f32[8,32,4,128]{3,0,2,1:T(8,128)S(1)} %get-tuple-element.336, s32[]{:T(128)S(6)} %copy.127), kind=kOutput, calls=%fused_computation.1.clone.1 | convolution fusion | flops 25165824 | bytes 8519684 | tf_op jit(solution)/shard_map/while/body/eval_jaxpr/shkv,shk->shv/dot_general | solution.py:54
  139.1 1.3 constant_dynamic-slice_fusion.10
  140.6 10.5 %add_select_fusion.4 = f32[32,4,128,128]{3,2,1,0:T(8,128)} fusion(f32[32,4,128,128]{3,2,1,0:T(8,128)} %get-tuple-element.320, f32[32,4,128]{2,1,0:T(4,128)S(1)} %bitcast.274, f32[32,4,128]{2,1,0:T(4,128)S(1)} %bitcast.275, f32[32,4,128]{2,1,0:T(4,128)S(1)} %exponential_bitcast_fusion.4, pred[32]{0:T(512)(128)(4,1)S(1)} %dynamic-slice_bitcast_fusion.4), kind=kLoop, calls=%fused_computation.clone.1 | loop fusion | flops 8388608 | bytes 16973856 | tf_op jit(solution)/shard_map/while/body/eval_jaxpr/jit(_where)/select_n | solution.py:53
  151.1 9.5 %convolution_bitcast_fusion.4 = f32[1,32,4,128]{3,0,2,1:T(1,128)S(1)} fusion(f32[32,4,128,128]{3,2,1,0:T(8,128)} %add_select_fusion.4, f32[8,32,4,128]{3,0,2,1:T(8,128)S(1)} %get-tuple-element.336, s32[]{:T(128)S(6)} %copy.127), kind=kOutput, calls=%fused_computation.1.clone.1 | convolution fusion | flops 25165824 | bytes 8519684 | tf_op jit(solution)/shard_map/while/body/eval_jaxpr/shkv,shk->shv/dot_general | solution.py:54
  162.0 1.3 constant_dynamic-slice_fusion.10
  163.5 10.5 %add_select_fusion.4 = f32[32,4,128,128]{3,2,1,0:T(8,128)} fusion(f32[32,4,128,128]{3,2,1,0:T(8,128)} %get-tuple-element.320, f32[32,4,128]{2,1,0:T(4,128)S(1)} %bitcast.274, f32[32,4,128]{2,1,0:T(4,128)S(1)} %bitcast.275, f32[32,4,128]{2,1,0:T(4,128)S(1)} %exponential_bitcast_fusion.4, pred[32]{0:T(512)(128)(4,1)S(1)} %dynamic-slice_bitcast_fusion.4), kind=kLoop, calls=%fused_computation.clone.1 | loop fusion | flops 8388608 | bytes 16973856 | tf_op jit(solution)/shard_map/while/body/eval_jaxpr/jit(_where)/select_n | solution.py:53
  174.0 9.5 %convolution_bitcast_fusion.4 = f32[1,32,4,128]{3,0,2,1:T(1,128)S(1)} fusion(f32[32,4,128,128]{3,2,1,0:T(8,128)} %add_select_fusion.4, f32[8,32,4,128]{3,0,2,1:T(8,128)S(1)} %get-tuple-element.336, s32[]{:T(128)S(6)} %copy.127), kind=kOutput, calls=%fused_computation.1.clone.1 | convolution fusion | flops 25165824 | bytes 8519684 | tf_op jit(solution)/shard_map/while/body/eval_jaxpr/shkv,shk->shv/dot_general | solution.py:54
  184.9 1.3 constant_dynamic-slice_fusion.10
  186.3 10.5 %add_select_fusion.4 = f32[32,4,128,128]{3,2,1,0:T(8,128)} fusion(f32[32,4,128,128]{3,2,1,0:T(8,128)} %get-tuple-element.320, f32[32,4,128]{2,1,0:T(4,128)S(1)} %bitcast.274, f32[32,4,128]{2,1,0:T(4,128)S(1)} %bitcast.275, f32[32,4,128]{2,1,0:T(4,128)S(1)} %exponential_bitcast_fusion.4, pred[32]{0:T(512)(128)(4,1)S(1)} %dynamic-slice_bitcast_fusion.4), kind=kLoop, calls=%fused_computation.clone.1 | loop fusion | flops 8388608 | bytes 16973856 | tf_op jit(solution)/shard_map/while/body/eval_jaxpr/jit(_where)/select_n | solution.py:53
  196.9 9.5 %convolution_bitcast_fusion.4 = f32[1,32,4,128]{3,0,2,1:T(1,128)S(1)} fusion(f32[32,4,128,128]{3,2,1,0:T(8,128)} %add_select_fusion.4, f32[8,32,4,128]{3,0,2,1:T(8,128)S(1)} %get-tuple-element.336, s32[]{:T(128)S(6)} %copy.127), kind=kOutput, calls=%fused_computation.1.clone.1 | convolution fusion | flops 25165824 | bytes 8519684 | tf_op jit(solution)/shard_map/while/body/eval_jaxpr/shkv,shk->shv/dot_general | solution.py:54
  207.8 1.3 constant_dynamic-slice_fusion.10
  209.2 10.5 %add_select_fusion.4 = f32[32,4,128,128]{3,2,1,0:T(8,128)} fusion(f32[32,4,128,128]{3,2,1,0:T(8,128)} %get-tuple-element.320, f32[32,4,128]{2,1,0:T(4,128)S(1)} %bitcast.274, f32[32,4,128]{2,1,0:T(4,128)S(1)} %bitcast.275, f32[32,4,128]{2,1,0:T(4,128)S(1)} %exponential_bitcast_fusion.4, pred[32]{0:T(512)(128)(4,1)S(1)} %dynamic-slice_bitcast_fusion.4), kind=kLoop, calls=%fused_computation.clone.1 | loop fusion | flops 8388608 | bytes 16973856 | tf_op jit(solution)/shard_map/while/body/eval_jaxpr/jit(_where)/select_n | solution.py:53
  219.7 9.5 %convolution_bitcast_fusion.4 = f32[1,32,4,128]{3,0,2,1:T(1,128)S(1)} fusion(f32[32,4,128,128]{3,2,1,0:T(8,128)} %add_select_fusion.4, f32[8,32,4,128]{3,0,2,1:T(8,128)S(1)} %get-tuple-element.336, s32[]{:T(128)S(6)} %copy.127), kind=kOutput, calls=%fused_computation.1.clone.1 | convolution fusion | flops 25165824 | bytes 8519684 | tf_op jit(solution)/shard_map/while/body/eval_jaxpr/shkv,shk->shv/dot_general | solution.py:54
  232.1 10.5 %add_select_fusion.4 = f32[32,4,128,128]{3,2,1,0:T(8,128)} fusion(f32[32,4,128,128]{3,2,1,0:T(8,128)} %get-tuple-element.320, f32[32,4,128]{2,1,0:T(4,128)S(1)} %bitcast.274, f32[32,4,128]{2,1,0:T(4,128)S(1)} %bitcast.275, f32[32,4,128]{2,1,0:T(4,128)S(1)} %exponential_bitcast_fusion.4, pred[32]{0:T(512)(128)(4,1)S(1)} %dynamic-slice_bitcast_fusion.4), kind=kLoop, calls=%fused_computation.clone.1 | loop fusion | flops 8388608 | bytes 16973856 | tf_op jit(solution)/shard_map/while/body/eval_jaxpr/jit(_where)/select_n | solution.py:53
  242.6 9.5 %convolution_bitcast_fusion.4 = f32[1,32,4,128]{3,0,2,1:T(1,128)S(1)} fusion(f32[32,4,128,128]{3,2,1,0:T(8,128)} %add_select_fusion.4, f32[8,32,4,128]{3,0,2,1:T(8,128)S(1)} %get-tuple-element.336, s32[]{:T(128)S(6)} %copy.127), kind=kOutput, calls=%fused_computation.1.clone.1 | convolution fusion | flops 25165824 | bytes 8519684 | tf_op jit(solution)/shard_map/while/body/eval_jaxpr/shkv,shk->shv/dot_general | solution.py:54
  255.0 16.8 %all-gather.3.cloned.1.call-done = bf16[1024,512]{1,0:T(8,128)(2,1)} async-done(((bf16[256,512]{1,0:T(8,128)(2,1)}), bf16[1024,512]{1,0:T(8,128)(2,1)}) %all-gather.3.cloned.1.call-update) | async-done | bytes 1048592 | tf_op jit(solution)/shard_map/all_gather | solution.py:144
  271.8 4.1 convolution_convert_fusion.1
  276.2 102.2 %all-reduce.3.cloned.1.call-done = bf16[1024,1024]{1,0:T(8,128)(2,1)} async-done(((bf16[1024,1024]{1,0:T(8,128)(2,1)}), bf16[1024,1024]{1,0:T(8,128)(2,1)}) %all-reduce.3.cloned.1.call-update) | async-done | bytes 2097168 | tf_op jit(solution)/shard_map/psum | solution.py:148
  378.4 3.0 fusion.10
  381.4 2.7 convolution_convert_fusion.2
  388.6 2.3 pad_maximum_fusion.2
  391.1 6.1 psum.30
  397.4 37.4 %reduce-scatter.5.cloned.1.call-done = bf16[256,2048]{0,1:T(8,128)(2,1)} async-done(((bf16[1024,2048]{0,1:T(8,128)(2,1)}), bf16[256,2048]{0,1:T(8,128)(2,1)}) %reduce-scatter.5.cloned.1.call-update) | async-done | bytes 1048592 | tf_op jit(solution)/shard_map/reduce_scatter | solution.py:119
  434.7 1.4 multiply_convert_fusion
  439.7 2.0 copy.91
  442.7 2.0 copy.92
  447.0 2.4 fusion.61
  449.4 191.7 %while.25 = (s32[]{:T(128)}, f32[32,4,128,128]{3,2,1,0:T(8,128)}, f32[8,32,4,128]{3,0,2,1:T(8,128)S(1)}, pred[8,32]{1,0:T(8,128)(4,1)S(1)}, f32[8,32,4,128]{3,0,...) while((s32[]{:T(128)}, f32[32,4,128,128]{3,2,1,0:T(8,128)}, ...), condition=%wide.region_11.12_spmd, body=%wide.region_10.11_spmd.sunk | while | flops 33554432 | bytes 26149088 | solution.py:57
  451.9 10.6 %add_select_fusion.5 = f32[32,4,128,128]{3,2,1,0:T(8,128)} fusion(f32[32,4,128,128]{3,2,1,0:T(8,128)} %get-tuple-element.350, f32[32,4,128]{2,1,0:T(4,128)S(1)} %bitcast.276, f32[32,4,128]{2,1,0:T(4,128)S(1)} %bitcast.277, f32[32,4,128]{2,1,0:T(4,128)S(1)} %exponential_bitcast_fusion.5, pred[32]{0:T(512)(128)(4,1)S(1)} %dynamic-slice_bitcast_fusion.5), kind=kLoop, calls=%fused_computation.10.clone.1 | loop fusion | flops 8388608 | bytes 16973856 | tf_op jit(solution)/shard_map/while/body/eval_jaxpr/jit(_where)/select_n | solution.py:53
  462.4 9.6 %convolution_bitcast_fusion.5 = f32[1,32,4,128]{3,0,2,1:T(1,128)S(1)} fusion(f32[32,4,128,128]{3,2,1,0:T(8,128)} %add_select_fusion.5, f32[8,32,4,128]{3,0,2,1:T(8,128)} %get-tuple-element.366, s32[]{:T(128)S(6)} %copy.137), kind=kOutput, calls=%fused_computation.11.clone.1 | convolution fusion | flops 25165824 | bytes 8519684 | tf_op jit(solution)/shard_map/while/body/eval_jaxpr/shkv,shk->shv/dot_general | solution.py:54
  475.8 10.6 %add_select_fusion.5 = f32[32,4,128,128]{3,2,1,0:T(8,128)} fusion(f32[32,4,128,128]{3,2,1,0:T(8,128)} %get-tuple-element.350, f32[32,4,128]{2,1,0:T(4,128)S(1)} %bitcast.276, f32[32,4,128]{2,1,0:T(4,128)S(1)} %bitcast.277, f32[32,4,128]{2,1,0:T(4,128)S(1)} %exponential_bitcast_fusion.5, pred[32]{0:T(512)(128)(4,1)S(1)} %dynamic-slice_bitcast_fusion.5), kind=kLoop, calls=%fused_computation.10.clone.1 | loop fusion | flops 8388608 | bytes 16973856 | tf_op jit(solution)/shard_map/while/body/eval_jaxpr/jit(_where)/select_n | solution.py:53
  486.4 9.6 %convolution_bitcast_fusion.5 = f32[1,32,4,128]{3,0,2,1:T(1,128)S(1)} fusion(f32[32,4,128,128]{3,2,1,0:T(8,128)} %add_select_fusion.5, f32[8,32,4,128]{3,0,2,1:T(8,128)} %get-tuple-element.366, s32[]{:T(128)S(6)} %copy.137), kind=kOutput, calls=%fused_computation.11.clone.1 | convolution fusion | flops 25165824 | bytes 8519684 | tf_op jit(solution)/shard_map/while/body/eval_jaxpr/shkv,shk->shv/dot_general | solution.py:54
  499.8 10.6 %add_select_fusion.5 = f32[32,4,128,128]{3,2,1,0:T(8,128)} fusion(f32[32,4,128,128]{3,2,1,0:T(8,128)} %get-tuple-element.350, f32[32,4,128]{2,1,0:T(4,128)S(1)} %bitcast.276, f32[32,4,128]{2,1,0:T(4,128)S(1)} %bitcast.277, f32[32,4,128]{2,1,0:T(4,128)S(1)} %exponential_bitcast_fusion.5, pred[32]{0:T(512)(128)(4,1)S(1)} %dynamic-slice_bitcast_fusion.5), kind=kLoop, calls=%fused_computation.10.clone.1 | loop fusion | flops 8388608 | bytes 16973856 | tf_op jit(solution)/shard_map/while/body/eval_jaxpr/jit(_where)/select_n | solution.py:53
  510.4 9.6 %convolution_bitcast_fusion.5 = f32[1,32,4,128]{3,0,2,1:T(1,128)S(1)} fusion(f32[32,4,128,128]{3,2,1,0:T(8,128)} %add_select_fusion.5, f32[8,32,4,128]{3,0,2,1:T(8,128)} %get-tuple-element.366, s32[]{:T(128)S(6)} %copy.137), kind=kOutput, calls=%fused_computation.11.clone.1 | convolution fusion | flops 25165824 | bytes 8519684 | tf_op jit(solution)/shard_map/while/body/eval_jaxpr/shkv,shk->shv/dot_general | solution.py:54
  523.7 10.6 %add_select_fusion.5 = f32[32,4,128,128]{3,2,1,0:T(8,128)} fusion(f32[32,4,128,128]{3,2,1,0:T(8,128)} %get-tuple-element.350, f32[32,4,128]{2,1,0:T(4,128)S(1)} %bitcast.276, f32[32,4,128]{2,1,0:T(4,128)S(1)} %bitcast.277, f32[32,4,128]{2,1,0:T(4,128)S(1)} %exponential_bitcast_fusion.5, pred[32]{0:T(512)(128)(4,1)S(1)} %dynamic-slice_bitcast_fusion.5), kind=kLoop, calls=%fused_computation.10.clone.1 | loop fusion | flops 8388608 | bytes 16973856 | tf_op jit(solution)/shard_map/while/body/eval_jaxpr/jit(_where)/select_n | solution.py:53
  534.3 9.6 %convolution_bitcast_fusion.5 = f32[1,32,4,128]{3,0,2,1:T(1,128)S(1)} fusion(f32[32,4,128,128]{3,2,1,0:T(8,128)} %add_select_fusion.5, f32[8,32,4,128]{3,0,2,1:T(8,128)} %get-tuple-element.366, s32[]{:T(128)S(6)} %copy.137), kind=kOutput, calls=%fused_computation.11.clone.1 | convolution fusion | flops 25165824 | bytes 8519684 | tf_op jit(solution)/shard_map/while/body/eval_jaxpr/shkv,shk->shv/dot_general | solution.py:54
  547.7 10.6 %add_select_fusion.5 = f32[32,4,128,128]{3,2,1,0:T(8,128)} fusion(f32[32,4,128,128]{3,2,1,0:T(8,128)} %get-tuple-element.350, f32[32,4,128]{2,1,0:T(4,128)S(1)} %bitcast.276, f32[32,4,128]{2,1,0:T(4,128)S(1)} %bitcast.277, f32[32,4,128]{2,1,0:T(4,128)S(1)} %exponential_bitcast_fusion.5, pred[32]{0:T(512)(128)(4,1)S(1)} %dynamic-slice_bitcast_fusion.5), kind=kLoop, calls=%fused_computation.10.clone.1 | loop fusion | flops 8388608 | bytes 16973856 | tf_op jit(solution)/shard_map/while/body/eval_jaxpr/jit(_where)/select_n | solution.py:53
  558.3 9.6 %convolution_bitcast_fusion.5 = f32[1,32,4,128]{3,0,2,1:T(1,128)S(1)} fusion(f32[32,4,128,128]{3,2,1,0:T(8,128)} %add_select_fusion.5, f32[8,32,4,128]{3,0,2,1:T(8,128)} %get-tuple-element.366, s32[]{:T(128)S(6)} %copy.137), kind=kOutput, calls=%fused_computation.11.clone.1 | convolution fusion | flops 25165824 | bytes 8519684 | tf_op jit(solution)/shard_map/while/body/eval_jaxpr/shkv,shk->shv/dot_general | solution.py:54
  571.7 10.6 %add_select_fusion.5 = f32[32,4,128,128]{3,2,1,0:T(8,128)} fusion(f32[32,4,128,128]{3,2,1,0:T(8,128)} %get-tuple-element.350, f32[32,4,128]{2,1,0:T(4,128)S(1)} %bitcast.276, f32[32,4,128]{2,1,0:T(4,128)S(1)} %bitcast.277, f32[32,4,128]{2,1,0:T(4,128)S(1)} %exponential_bitcast_fusion.5, pred[32]{0:T(512)(128)(4,1)S(1)} %dynamic-slice_bitcast_fusion.5), kind=kLoop, calls=%fused_computation.10.clone.1 | loop fusion | flops 8388608 | bytes 16973856 | tf_op jit(solution)/shard_map/while/body/eval_jaxpr/jit(_where)/select_n | solution.py:53
  582.2 9.6 %convolution_bitcast_fusion.5 = f32[1,32,4,128]{3,0,2,1:T(1,128)S(1)} fusion(f32[32,4,128,128]{3,2,1,0:T(8,128)} %add_select_fusion.5, f32[8,32,4,128]{3,0,2,1:T(8,128)} %get-tuple-element.366, s32[]{:T(128)S(6)} %copy.137), kind=kOutput, calls=%fused_computation.11.clone.1 | convolution fusion | flops 25165824 | bytes 8519684 | tf_op jit(solution)/shard_map/while/body/eval_jaxpr/shkv,shk->shv/dot_general | solution.py:54
  595.6 10.6 %add_select_fusion.5 = f32[32,4,128,128]{3,2,1,0:T(8,128)} fusion(f32[32,4,128,128]{3,2,1,0:T(8,128)} %get-tuple-element.350, f32[32,4,128]{2,1,0:T(4,128)S(1)} %bitcast.276, f32[32,4,128]{2,1,0:T(4,128)S(1)} %bitcast.277, f32[32,4,128]{2,1,0:T(4,128)S(1)} %exponential_bitcast_fusion.5, pred[32]{0:T(512)(128)(4,1)S(1)} %dynamic-slice_bitcast_fusion.5), kind=kLoop, calls=%fused_computation.10.clone.1 | loop fusion | flops 8388608 | bytes 16973856 | tf_op jit(solution)/shard_map/while/body/eval_jaxpr/jit(_where)/select_n | solution.py:53
  606.2 9.6 %convolution_bitcast_fusion.5 = f32[1,32,4,128]{3,0,2,1:T(1,128)S(1)} fusion(f32[32,4,128,128]{3,2,1,0:T(8,128)} %add_select_fusion.5, f32[8,32,4,128]{3,0,2,1:T(8,128)} %get-tuple-element.366, s32[]{:T(128)S(6)} %copy.137), kind=kOutput, calls=%fused_computation.11.clone.1 | convolution fusion | flops 25165824 | bytes 8519684 | tf_op jit(solution)/shard_map/while/body/eval_jaxpr/shkv,shk->shv/dot_general | solution.py:54
  619.6 10.6 %add_select_fusion.5 = f32[32,4,128,128]{3,2,1,0:T(8,128)} fusion(f32[32,4,128,128]{3,2,1,0:T(8,128)} %get-tuple-element.350, f32[32,4,128]{2,1,0:T(4,128)S(1)} %bitcast.276, f32[32,4,128]{2,1,0:T(4,128)S(1)} %bitcast.277, f32[32,4,128]{2,1,0:T(4,128)S(1)} %exponential_bitcast_fusion.5, pred[32]{0:T(512)(128)(4,1)S(1)} %dynamic-slice_bitcast_fusion.5), kind=kLoop, calls=%fused_computation.10.clone.1 | loop fusion | flops 8388608 | bytes 16973856 | tf_op jit(solution)/shard_map/while/body/eval_jaxpr/jit(_where)/select_n | solution.py:53
  630.2 9.6 %convolution_bitcast_fusion.5 = f32[1,32,4,128]{3,0,2,1:T(1,128)S(1)} fusion(f32[32,4,128,128]{3,2,1,0:T(8,128)} %add_select_fusion.5, f32[8,32,4,128]{3,0,2,1:T(8,128)} %get-tuple-element.366, s32[]{:T(128)S(6)} %copy.137), kind=kOutput, calls=%fused_computation.11.clone.1 | convolution fusion | flops 25165824 | bytes 8519684 | tf_op jit(solution)/shard_map/while/body/eval_jaxpr/shkv,shk->shv/dot_general | solution.py:54
  642.5 16.8 %all-gather.5.cloned.1.call-done = bf16[1024,512]{1,0:T(8,128)(2,1)} async-done(((bf16[256,512]{1,0:T(8,128)(2,1)}), bf16[1024,512]{1,0:T(8,128)(2,1)}) %all-gather.5.cloned.1.call-update) | async-done | bytes 1048592 | tf_op jit(solution)/shard_map/all_gather | solution.py:144
  659.4 4.1 convolution_convert_fusion
  663.5 11.9 %pad_maximum_fusion = f32[2,32,4,128,128]{4,3,2,1,0:T(8,128)} fusion(f32[1,32,4,128,128]{4,3,2,1,0:T(8,128)} %bitcast.272, f32[1,32,4,128,128]{4,3,2,1,0:T(8,128)} %bitcast.273), kind=kLoop, calls=%fused_computation.20 | loop fusion | flops 4194304 | bytes 33554432 | tf_op jit(solution)/shard_map/stack | solution.py:150
  675.5 90.5 %all-reduce.5.cloned.1.call-done = bf16[1024,1024]{1,0:T(8,128)(2,1)} async-done(((bf16[1024,1024]{1,0:T(8,128)(2,1)}), bf16[1024,1024]{1,0:T(8,128)(2,1)}) %all-reduce.5.cloned.1.call-update) | async-done | bytes 2097168 | tf_op jit(solution)/shard_map/psum | solution.py:148
  765.9 3.9 fusion.11
  (156 shorter events, 67.8 us)
Async XLA Ops:
  7.2 4.5 copy-start
  7.2 58.5 %reduce-scatter.3.cloned.1.call-start = ((), (), s32[]{:S(2)}) async-start(), calls=%async_computation.2 | async-start | bytes 5242880 | tf_op jit(solution)/shard_map/reduce_scatter | solution.py:119
  7.2 4.4 copy-start.5
  11.6 1.6 copy-start.7
  13.2 1.6 copy-start.9
  18.4 0.7 copy-start.1
  18.4 9.8 %copy-start.4 = (s32[32]{0:T(128)S(1)}, s32[32]{0:T(128)}, u32[]{:S(2)}) copy-start(s32[32]{0:T(128)} %param.17) | copy-start | bytes 388
  18.4 9.8 %copy-start.2 = (f32[2,512]{1,0:T(2,128)S(1)}, f32[2,512]{1,0:T(2,128)}, u32[]{:S(2)}) copy-start(f32[2,512]{1,0:T(2,128)} %param.23) | copy-start | bytes 12292
  18.4 9.8 %copy-start.3 = (f32[2,512]{1,0:T(2,128)S(1)}, f32[2,512]{1,0:T(2,128)}, u32[]{:S(2)}) copy-start(f32[2,512]{1,0:T(2,128)} %param.25) | copy-start | bytes 12292
  18.4 253.4 %all-gather.3.cloned.1.call-start = ((), (), s32[]{:S(2)}) async-start(), calls=%async_computation.3 | async-start | bytes 1310720 | tf_op jit(solution)/shard_map/all_gather | solution.py:144
  254.9 123.4 %all-reduce.3.cloned.1.call-start = ((), (), s32[]{:S(2)}) async-start(), calls=%async_computation.4 | async-start | bytes 4194304 | tf_op jit(solution)/shard_map/psum | solution.py:148
  275.9 158.8 %reduce-scatter.5.cloned.1.call-start = ((), (), s32[]{:S(2)}) async-start(), calls=%async_computation.5 | async-start | bytes 5242880 | tf_op jit(solution)/shard_map/reduce_scatter | solution.py:119
  381.4 2.7 copy-start.6
  384.1 1.6 copy-start.8
  385.7 1.6 copy-start.10
  390.9 268.5 %all-gather.5.cloned.1.call-start = ((), (), s32[]{:S(2)}) async-start(), calls=%async_computation.6 | async-start | bytes 1310720 | tf_op jit(solution)/shard_map/all_gather | solution.py:144
  642.5 123.4 %all-reduce.5.cloned.1.call-start = ((), (), s32[]{:S(2)}) async-start(), calls=%async_computation.7 | async-start | bytes 4194304 | tf_op jit(solution)/shard_map/psum | solution.py:148
Sparse Core Ops, SparseCore 0:
  18.5 47.1 reduce-scatter.2
  255.1 16.6 all-gather.2
  276.1 102.2 all-reduce.2
  391.0 43.6 reduce-scatter.4
  642.6 16.7 all-gather.4
  663.6 102.2 all-reduce.4
where the time goes:
time: 781 us; the launch traced here: 777 us
  waiting for transfers between devices  289 us (37%)
  other arithmetic  205 us (26%)
  matrix products  175 us (22%)
  local copies, waits for them, and re-layouts  77.5 us (10%)
  blocking collectives  14.5 us (2%)
  between operations  14.5 us (2%)
    psum x2, waiting for transfers between devices, local(): update = lax.psum(partial_value.astype(jnp.bfloat16), 'tp')  193 us
    select_n x16, other arithmetic, advance(): matrix = jnp.where(live_now[:, None, None, None], updated, matrix)  169 us
    dot_general x16, matrix products, advance(): jnp.einsum('shkv,shk->shv', matrix, query_now, precision=lax.Precision.HI...  153 us
    reduce_scatter x2, waiting for transfers between devices, local(): lax.psum_scatter(project().astype(jnp.bfloat16), 'dp', scatter_dimension=...  62.5 us
    all_gather x2, waiting for transfers between devices, local(): lax.all_gather(attention_yields, 'dp', axis=0, tiled=True)  33.6 us
    dynamic_slice x32, local copies, waits for them, and re-layouts, update_tick(): lax.scan(advance, memory_grid, (jnp.moveaxis(queries, 1, 0), jnp.moveaxis...  30.5 us
    dynamic_update_slice x16, local copies, waits for them, and re-layouts, update_tick(): lax.scan(advance, memory_grid, (jnp.moveaxis(queries, 1, 0), jnp.moveaxis...  21.2 us
  transfers between devices with their start and end apart: 6, of which 6 were waited for; matrix products, arithmetic and copies ran while one was open for 3% of the time, Pallas kernels for 0%

commit v1 on v0

v1 whole, which is shorter than its diff:
```python
import functools

import jax
import jax.numpy as jnp
from jax import lax
from jax.experimental import pallas as pl
from jax.experimental.pallas import tpu as pltpu
from jax.sharding import PartitionSpec as P

EPSILON = 1e-05
F32, BF16 = jnp.float32, jnp.bfloat16
MESH = pl.DeviceIdType.MESH
LIVE_PER_SEQUENCE = 3
GROUP = 8
VMEM_LIMIT = 62 * 1024 * 1024


def peer(axis, offset):
    size = lax.axis_size(axis)
    return lax.rem(lax.axis_index(axis) + offset, size)


def aligned(start):
    return pl.multiple_of(start, 16)


def comm_kernel(sizes, has_out, layer, *refs):
    n, t, rows, live, feats, chans = sizes
    refs = list(refs)
    take = lambda: refs.pop(0)
    posrow_ref = take()
    if has_out:
        ho_ref, xc_in, we_ref = take(), take(), take()
    else:
        x_ref = take()
    if layer is not None:
        poscol_ref, gain_ref = take(), take()
        w_refs = [take() for _ in range(4)]
        z_ref = take()
    xc_out = take()
    if has_out:
        we_buf, we_sem = take(), take()
        hg, h_send, h_recv = take(), take(), take()
        h_fsend, h_frecv, upart, ufull = take(), take(), take(), take()
        halves = [[take() for _ in range(11)] for _ in range(2)]
    if layer is not None:
        w_buf, w_sem = take(), take()
        nb, part, pair_recv, x_send, x_recv, full = (take() for _ in range(6))
        pair_s, pair_r, xs, xr, ag_s, ag_r, fw_s, fw_r = (take() for _ in range(8))
        ssq, ssq_recv, sq_s, sq_r = take(), take(), take(), take()
    me, mt = lax.axis_index("dp"), lax.axis_index("tp")
    own = rows // n
    chips = n // 2
    chip, core = me // 2, lax.rem(me, 2)
    partner = chip * 2 + 1 - core

    def beside(k):
        return lax.rem(chip + k, chips) * 2 + core

    if has_out:
        we_copy = pltpu.make_async_copy(we_ref.at[(layer - 1) if layer is not None else 1], we_buf, we_sem)
        we_copy.start()
    if layer is not None:
        w_copies = [
            pltpu.make_async_copy(w_refs[w].at[layer], w_buf.at[w], w_sem.at[w]) for w in range(4)
        ]
        for copy in w_copies:
            copy.start()
    barrier = pltpu.get_barrier_semaphore()
    for k in range(1, n):
        pl.semaphore_signal(barrier, inc=1, device_id={"dp": peer("dp", k)}, device_id_type=MESH)
    if has_out:
        for k in range(1, t):
            pl.semaphore_signal(
                barrier, inc=1, device_id={"tp": peer("tp", k)}, device_id_type=MESH
            )
    expected = n - 1 + (t - 1 if has_out else 0)
    pending = []

    def remote(src, dst, send, recv, axis, target):
        return pltpu.make_async_remote_copy(
            src_ref=src, dst_ref=dst, send_sem=send, recv_sem=recv,
            device_id={axis: target}, device_id_type=MESH,
        )

    step = 128
    if has_out:
        pl.semaphore_wait(barrier, expected)
        copies = []
        for k in range(chips):
            target = partner if k == 0 else beside(k)
            copy = remote(ho_ref, hg.at[me], h_send.at[k], h_recv.at[k], "dp", target)
            copy.start()
            copies.append(copy)
        hg[me] = ho_ref[...]
        forwards = []
        for k in range(1, chips):
            copies[k].wait_recv()
            source = beside(chips - k)
            copy = remote(
                hg.at[source], hg.at[source], h_fsend.at[k - 1], h_frecv.at[k - 1], "dp", partner
            )
            copy.start()
            forwards.append(copy)
        we_copy.wait()
        copies[0].wait_recv()
        for copy in forwards:
            copy.wait_recv()
        pending += copies + forwards
        gathered = hg[...].reshape(rows, chans)
        for i in range(live // step):
            pick = (
                lax.broadcasted_iota(jnp.int32, (step, rows), 0) + i * step == posrow_ref[...]
            ).astype(F32).astype(BF16)
            hc = jnp.dot(pick, gathered, preferred_element_type=F32).astype(BF16)
            upart[pl.ds(i * step, step), :] = jnp.dot(
                hc, we_buf[...], preferred_element_type=F32
            ).astype(BF16)
        deep = 4 if t % 4 == 0 else 1
        flat = t // deep
        iz, iy = mt // flat, lax.rem(mt, flat)
        along_y = (flat, iy, lambda j: iz * flat + j)
        along_z = (deep, iz, lambda j: j * flat + iy)
        plans = [(along_y, along_z), (along_z, along_y)]
        width = feats // 2
        fine = live // t

        def send(group, src, dst, send_sem, recv_sem, target):
            copy = remote(src, dst, send_sem, recv_sem, "tp", target)
            copy.start()
            group.append(copy)

        def start(half, stage):
            (s1, i1, to1), (s2, i2, to2) = plans[half]
            r1, t1, r2, *sems = halves[half]
            s_sem, r_sem = sems[2 * stage], sems[2 * stage + 1]
            cols = pl.ds(half * width, width)
            coarse = live // s1
            block = pl.ds(aligned(i1 * coarse), coarse)
            mine = pl.ds(aligned(i1 * coarse + i2 * fine), fine)
            size, index, to = ((s1, i1, to1), (s2, i2, to2))[stage in (1, 2)]
            group = []
            for k in range(1, size):
                j = lax.rem(index + k, size)
                if stage == 0:
                    src = upart.at[pl.ds(aligned(j * coarse), coarse), cols]
                    dst = r1.at[k - 1]
                elif stage == 1:
                    src, dst = t1.at[pl.ds(aligned(j * fine), fine)], r2.at[k - 1]
                else:
                    where = mine if stage == 2 else block
                    src = dst = ufull.at[where, cols]
                send(group, src, dst, s_sem.at[k - 1], r_sem.at[k - 1], to(j))
            return group

        def finish(half, stage, group):
            (s1, i1, _), (s2, i2, _) = plans[half]
            r1, t1, r2 = halves[half][:3]
            cols = pl.ds(half * width, width)
            coarse = live // s1
            for copy in group:
                copy.wait_recv()
            if stage == 0:
                total = upart[pl.ds(aligned(i1 * coarse), coarse), cols].astype(F32)
                for k in range(s1 - 1):
                    total = total + r1[k].astype(F32)
                t1[...] = total.astype(BF16)
            elif stage == 1:
                total = t1[pl.ds(aligned(i2 * fine), fine), :].astype(F32)
                for k in range(s2 - 1):
                    total = total + r2[k].astype(F32)
                mine = pl.ds(aligned(i1 * coarse + i2 * fine), fine)
                ufull[mine, cols] = total.astype(BF16)
            return group

        groups = [start(half, 0) for half in range(2)]
        for stage in range(4):
            for half in range(2):
                pending += finish(half, stage, groups[half])
                if stage < 3:
                    groups[half] = start(half, stage + 1)
    for i in range(live // step):
        span = pl.ds(i * step, step)
        if has_out:
            cur = (xc_in[span, :].astype(F32) + ufull[span, :].astype(F32)).astype(BF16)
        else:
            pick = (
                lax.broadcasted_iota(jnp.int32, (step, rows), 0) + i * step == posrow_ref[...]
            ).astype(F32).astype(BF16)
            cur = jnp.dot(pick, x_ref[...], preferred_element_type=F32).astype(BF16)
        xc_out[span, :] = cur
        if layer is not None:
            cur = cur.astype(F32)
            nb[span, :] = (cur * gain_ref[layer : layer + 1, :]).astype(BF16)
            squares = jnp.sum(cur * cur, axis=1, keepdims=True)
            hi = squares.astype(BF16).astype(F32)
            mid = (squares - hi).astype(BF16).astype(F32)
            low = squares - hi - mid
            lane = lax.broadcasted_iota(jnp.int32, (step, 128), 1)
            ssq[span, :] = jnp.where(
                lane == 0, hi, jnp.where(lane == 1, mid, jnp.where(lane == 2, low, 0.0))
            ).astype(BF16)
    if layer is not None:
        if not has_out:
            pl.semaphore_wait(barrier, expected)
        chunk = live // n
        mine = pl.ds(aligned(me * chunk), chunk)
        sq_copies = []
        for k in range(1, n):
            src = pl.ds(aligned(peer("dp", k) * chunk), chunk)
            copy = remote(
                ssq.at[src], ssq_recv.at[k - 1], sq_s.at[k - 1], sq_r.at[k - 1],
                "dp", peer("dp", k),
            )
            copy.start()
            sq_copies.append(copy)
        pairs, crossings = [], []

        def chunk_of(index, side):
            return pl.ds(aligned((index * 2 + side) * chunk), chunk)

        def cross(w):
            group = []
            for k in range(1, chips):
                pairs[w][k].wait_recv()
                rows_k = chunk_of(lax.rem(chip + k, chips), core)
                x_send[w, k - 1] = (
                    part[w, rows_k, :].astype(F32) + pair_recv[w, k].astype(F32)
                ).astype(BF16)
                copy = remote(
                    x_send.at[w, k - 1], x_recv.at[w, k - 1], xs.at[w, k - 1], xr.at[w, k - 1],
                    "dp", beside(k),
                )
                copy.start()
                group.append(copy)
            crossings.append(group)

        for w in range(4):
            w_copies[w].wait()
            part[w] = jnp.dot(nb[...], w_buf[w], preferred_element_type=F32).astype(BF16)
            group = []
            for k in range(chips):
                src = chunk_of(lax.rem(chip + k, chips), 1 - core)
                copy = remote(
                    part.at[w, src], pair_recv.at[w, k], pair_s.at[w, k], pair_r.at[w, k],
                    "dp", partner,
                )
                copy.start()
                group.append(copy)
            pairs.append(group)
            if w > 0:
                cross(w - 1)
        cross(3)
        squares = jnp.sum(ssq[mine, :].astype(F32), axis=1, keepdims=True)
        for k in range(1, n):
            sq_copies[k - 1].wait_recv()
            squares = squares + jnp.sum(ssq_recv[k - 1].astype(F32), axis=1, keepdims=True)
        scale = lax.rsqrt(squares / (feats * n) + EPSILON)
        ag = []
        for w in range(4):
            pairs[w][0].wait_recv()
            total = part[w, mine, :].astype(F32) + pair_recv[w, 0].astype(F32)
            for k in range(1, chips):
                crossings[w][k - 1].wait_recv()
                total = total + x_recv[w, k - 1].astype(F32)
            full[w, mine, :] = (total * scale).astype(BF16)
            group = []
            for k in [*range(1, chips), 0]:
                copy = remote(
                    full.at[w, mine], full.at[w, mine], ag_s.at[w, k], ag_r.at[w, k],
                    "dp", partner if k == 0 else beside(k),
                )
                copy.start()
                group.append(copy)
            ag.append(group)
        forwards = []
        for w in range(4):
            group = []
            for k in range(1, chips):
                ag[w][k - 1].wait_recv()
                block = chunk_of(lax.rem(chip + chips - k, chips), core)
                copy = remote(
                    full.at[w, block], full.at[w, block], fw_s.at[w, k - 1], fw_r.at[w, k - 1],
                    "dp", partner,
                )
                copy.start()
                group.append(copy)
            forwards.append(group)
        spread = (
            lax.broadcasted_iota(jnp.int32, (own, live), 1)
            == poscol_ref[pl.ds(aligned(me * own), own), :]
        ).astype(F32).astype(BF16)
        for w in range(4):
            ag[w][-1].wait_recv()
            for copy in forwards[w]:
                copy.wait_recv()
            z_ref[:, w * chans : (w + 1) * chans] = jnp.dot(
                spread, full[w], preferred_element_type=F32
            ).astype(BF16)
            pending += pairs[w] + crossings[w] + ag[w] + forwards[w]
        pending += sq_copies
    for copy in pending:
        copy.wait_send()


def comm_call(sizes, has_out, layer, collective_id, args):
    n, t, rows, live, feats, chans = sizes
    vmem, hbm = pl.BlockSpec(memory_space=pltpu.VMEM), pl.BlockSpec(memory_space=pl.ANY)
    dma = pltpu.SemaphoreType.DMA
    chips = n // 2
    in_specs = [vmem]
    in_specs += [vmem, vmem, hbm] if has_out else [vmem]
    out_shape, scratch = [], []
    if layer is not None:
        in_specs += [vmem, vmem] + [hbm] * 4
        out_shape.append(jax.ShapeDtypeStruct((rows // n, 4 * chans), BF16))
    out_shape.append(jax.ShapeDtypeStruct((live, feats), BF16))
    if has_out:
        scratch += [
            pltpu.VMEM((chans, feats), BF16), dma,
            pltpu.VMEM((n, rows // n, chans), BF16), dma((chips,)), dma((chips,)),
            dma((chips - 1,)), dma((chips - 1,)),
            pltpu.VMEM((live, feats), BF16),
            pltpu.VMEM((live, feats), BF16),
        ]
        deep = 4 if t % 4 == 0 else 1
        for s1, s2 in ((t // deep, deep), (deep, t // deep)):
            scratch += [
                pltpu.VMEM((s1 - 1, live // s1, feats // 2), BF16),
                pltpu.VMEM((live // s1, feats // 2), BF16),
                pltpu.VMEM((s2 - 1, live // t, feats // 2), BF16),
            ]
            for size in (s1, s2, s2, s1):
                scratch += [dma((size - 1,)), dma((size - 1,))]
    if layer is not None:
        chunk = live // n
        scratch += [
            pltpu.VMEM((4, feats, chans), BF16), dma((4,)),
            pltpu.VMEM((live, feats), BF16),
            pltpu.VMEM((4, live, chans), BF16),
            pltpu.VMEM((4, chips, chunk, chans), BF16),
            pltpu.VMEM((4, chips - 1, chunk, chans), BF16),
            pltpu.VMEM((4, chips - 1, chunk, chans), BF16),
            pltpu.VMEM((4, live, chans), BF16),
            dma((4, chips)), dma((4, chips)), dma((4, chips - 1)), dma((4, chips - 1)),
            dma((4, chips)), dma((4, chips)), dma((4, chips - 1)), dma((4, chips - 1)),
            pltpu.VMEM((live, 128), BF16),
            pltpu.VMEM((n - 1, chunk, 128), BF16),
            dma((n - 1,)), dma((n - 1,)),
        ]
    return pl.pallas_call(
        functools.partial(comm_kernel, sizes, has_out, layer),
        out_shape=out_shape,
        in_specs=in_specs,
        out_specs=[vmem] * len(out_shape),
        scratch_shapes=scratch,
        compiler_params=pltpu.CompilerParams(
            collective_id=collective_id, has_side_effects=True, vmem_limit_bytes=VMEM_LIMIT
        ),
        name=f"comm{collective_id}",
    )(*args)


def recurrence_kernel(layer, heads, new, z_ref, ext_ref, low_ref, gain_ref, s_ref, *rest):
    ho_ref, ns_ref = rest[-2:]
    group, width = s_ref.shape[1], s_ref.shape[3]
    chans = heads * width
    lines = group * new
    live = ext_ref[:, heads : heads + 1] > 0.5
    row = lax.broadcasted_iota(jnp.int32, (lines, width), 0)
    slot = lax.broadcasted_iota(jnp.int32, (group, new, width), 1)
    for h in range(heads):
        cols = slice(h * width, (h + 1) * width)

        def piece(w):
            start = w * chans + h * width
            return z_ref[:, start : start + width].astype(F32)

        query, forget, value, gate = (piece(w) for w in range(4))
        low = low_ref[layer : layer + 1, cols]
        query = query * jax.nn.sigmoid(query)
        decay = (low + (1.0 - low) * jax.nn.sigmoid(forget)) * jnp.exp(ext_ref[:, h : h + 1])
        key = (1.0 - low) * jax.nn.sigmoid(-forget)
        decay = jnp.where(live, decay, 1.0).reshape(group, new, width)
        key = jnp.where(live, key, 0.0).reshape(group, new, width)
        query = query.reshape(group, new, width)
        value3 = value.reshape(group, new, width)
        decayed = jnp.where(slot == 0, key, 0.0)
        total = decay[:, 0:1, :]
        carried = jnp.zeros_like(query)
        intra = jnp.zeros_like(query)
        for p in range(new):
            if p > 0:
                now = decay[:, p : p + 1, :]
                decayed = jnp.where(slot == p, key, decayed * now)
                total = total * now
            asked = query[:, p : p + 1, :]
            score = jnp.sum(asked * decayed, axis=2, keepdims=True)
            found = jnp.sum(score * value3, axis=1, keepdims=True)
            intra = jnp.where(slot == p, found, intra)
            carried = jnp.where(slot == p, asked * total, carried)
        stacked = jnp.concatenate(
            [
                decayed.reshape(lines, width),
                total.reshape(group, width),
                jnp.zeros((width - lines - group, width), F32),
            ],
            axis=0,
        )
        turned = stacked.T
        keys = turned[:, :lines].astype(BF16)
        reads = []
        for g in range(group):
            state = s_ref[0, g, h]
            reads.append(
                jnp.dot(
                    carried[g].astype(BF16), state.astype(BF16), preferred_element_type=F32
                )
            )
            mine = jnp.where(row // new == g, value, 0.0).astype(BF16)
            added = jnp.dot(keys, mine, preferred_element_type=F32)
            ns_ref[0, g, h] = turned[:, lines + g : lines + g + 1] * state + added
        read = jnp.concatenate(reads, axis=0) + intra.reshape(lines, width)
        scale = lax.rsqrt(jnp.mean(read * read, axis=1, keepdims=True) + EPSILON)
        out = read * scale * gain_ref[layer : layer + 1, cols] * (gate * jax.nn.sigmoid(gate))
        ho_ref[:, cols] = jnp.where(live, out, 0.0).astype(BF16)


def recurrence_call(layer, z, ext, low, gain, states, previous):
    blocks, seqs, heads, width, _ = states.shape
    new = z.shape[0] // seqs
    chans = heads * width
    lines = GROUP * new
    state_spec = pl.BlockSpec((1, GROUP, heads, width, width), lambda i: (layer, i, 0, 0, 0))
    in_specs = [
        pl.BlockSpec((lines, 4 * chans), lambda i: (i, 0)),
        pl.BlockSpec((lines, heads + 1), lambda i: (i, 0)),
        pl.BlockSpec((blocks, chans), lambda i: (0, 0)),
        pl.BlockSpec((blocks, chans), lambda i: (0, 0)),
        state_spec,
    ]
    args = [z, ext, low, gain, states]
    aliases = {}
    if previous is not None:
        in_specs.append(pl.BlockSpec(memory_space=pl.ANY))
        args.append(previous)
        aliases = {5: 1}
    return pl.pallas_call(
        functools.partial(recurrence_kernel, layer, heads, new),
        grid=(seqs // GROUP,),
        out_shape=[
            jax.ShapeDtypeStruct((z.shape[0], chans), BF16),
            jax.ShapeDtypeStruct(states.shape, F32),
        ],
        in_specs=in_specs,
        out_specs=[pl.BlockSpec((lines, chans), lambda i: (i, 0)), state_spec],
        input_output_aliases=aliases,
        compiler_params=pltpu.CompilerParams(
            dimension_semantics=("arbitrary",), vmem_limit_bytes=40 * 1024 * 1024
        ),
        name=f"recurrence{layer}",
    )(*args)


def local(
    activation_rows,
    fresh_spans,
    entry_rescale_vector,
    probe_kernel,
    retention_kernel,
    content_kernel,
    valve_kernel,
    retention_minimum,
    extra_attenuation,
    channel_rescale_vector,
    emission_kernel,
    memory_grids,
):
    n, t = lax.axis_size("dp"), lax.axis_size("tp")
    rows, feats = activation_rows.shape
    chans = probe_kernel.shape[2]
    own_seqs = fresh_spans.shape[0]
    seqs = own_seqs * n
    new = rows // seqs
    sizes = (n, t, rows, LIVE_PER_SEQUENCE * seqs, feats, chans)
    weights = (probe_kernel, retention_kernel, content_kernel, valve_kernel)

    spans = lax.all_gather(fresh_spans, "dp", axis=0, tiled=True)
    before = lax.broadcasted_iota(jnp.int32, (seqs, seqs), 1) < lax.broadcasted_iota(
        jnp.int32, (seqs, seqs), 0
    )
    starts = jnp.sum(jnp.where(before, spans[None, :], 0), axis=1)
    slots = lax.broadcasted_iota(jnp.int32, (seqs, new), 1)
    position = jnp.where(slots < spans[:, None], starts[:, None] + slots, -1).reshape(rows)
    posrow, poscol = position[None, :], position[:, None]
    own_live = (
        lax.broadcasted_iota(jnp.int32, (own_seqs, new), 1) < fresh_spans[:, None]
    ).reshape(own_seqs * new, 1)
    ext = [
        jnp.concatenate([extra_attenuation[b], own_live.astype(F32)], axis=1) for b in range(2)
    ]

    z, xc = comm_call(
        sizes, False, 0, 0, (posrow, activation_rows, poscol, entry_rescale_vector, *weights)
    )
    heads_out, states = recurrence_call(
        0, z, ext[0], retention_minimum, channel_rescale_vector, memory_grids, None
    )
    z, xc = comm_call(
        sizes, True, 1, 1,
        (posrow, heads_out, xc, emission_kernel, poscol, entry_rescale_vector, *weights),
    )
    heads_out, states = recurrence_call(
        1, z, ext[1], retention_minimum, channel_rescale_vector, memory_grids, states
    )
    (xc,) = comm_call(sizes, True, None, 2, (posrow, heads_out, xc, emission_kernel))
    spread = (
        lax.broadcasted_iota(jnp.int32, (rows, sizes[3]), 1) == poscol
    ).astype(BF16)
    moved = jnp.dot(spread, xc, preferred_element_type=F32).astype(BF16)
    mixed = jnp.where(poscol >= 0, moved, activation_rows)
    return (mixed, states)


def solution(mesh):
    placed = (
        P(None, "dp"),
        P("dp"),
        P(None, "dp"),
        P(None, "dp", "tp"),
        P(None, "dp", "tp"),
        P(None, "dp", "tp"),
        P(None, "dp", "tp"),
        P(None, "tp"),
        P(None, "dp", "tp"),
        P(None, "tp"),
        P(None, "tp", "dp"),
        P(None, "dp", "tp", None, None),
    )
    return jax.shard_map(
        local,
        mesh=mesh,
        in_specs=placed,
        out_specs=(P(None, "dp"), P(None, "dp", "tp", None, None)),
        check_vma=False,
    )
```

time: 781 us -> 186 us (0.24)
  waiting for transfers between devices: 289 us -> 0 us
  other arithmetic: 205 us -> 0.95 us
  matrix products: 175 us -> 4.25 us
  Pallas kernels: 0 us -> 163 us
  local copies, waits for them, and re-layouts: 77.5 us -> 8.78 us
  between operations: 14.5 us -> 1.4 us
  blocking collectives: 14.5 us -> 6.38 us
    psum x2 -> x0, waiting for transfers between devices: 193 us -> none  [local(): update = lax.psum(partial_value.astype(jnp.bfloat16), 'tp')]
    dot_general x26 -> x1, matrix products: 175 us -> 4.25 us  [local(): moved = jnp.dot(spread, xc, preferred_element_type=F32).astype(BF16)]
    select_n x16 -> x1, other arithmetic: 169 us -> 0.1 us  [local(): jnp.where(slots < spans[:, None], starts[:, None] + slots, -1).reshape(rows)]
    pallas_call x0 -> x5, Pallas kernels: none -> 163 us  [the longest x3 141 us: comm_call(): pl.pallas_call(functools.partial(comm_kernel, sizes, has_out, layer), out...]
    reduce_scatter x2 -> x0, waiting for transfers between devices: 62.5 us -> none  [local(): lax.psum_scatter(project().astype(jnp.bfloat16), 'dp', scatter_dimension=...]
    all_gather x2 -> x0, waiting for transfers between devices: 33.6 us -> none  [local(): lax.all_gather(attention_yields, 'dp', axis=0, tiled=True)]
    dynamic_slice x34 -> x0, local copies, waits for them, and re-layouts: 30.7 us -> none  [the longest x32 30.5 us: update_tick(): lax.scan(advance, memory_grid, (jnp.moveaxis(queries, 1, 0), jnp.moveaxis...]
    dynamic_update_slice x16 -> x0, local copies, waits for them, and re-layouts: 21.2 us -> none  [update_tick(): lax.scan(advance, memory_grid, (jnp.moveaxis(queries, 1, 0), jnp.moveaxis...]
  transfers between devices with their start and end apart: 6 -> 0, of which waited for: 6 -> 0; matrix products, arithmetic and copies ran while one was open for 3% -> 0% of each run, Pallas kernels for 0% -> 0%
where the time goes in v1:
time: 186 us; the launch traced here: 185 us
  Pallas kernels  163 us (88%)
  local copies, waits for them, and re-layouts  8.78 us (5%)
  blocking collectives  6.38 us (3%)
  matrix products  4.25 us (2%)
    pallas_call x3, Pallas kernels, comm_call(): pl.pallas_call(functools.partial(comm_kernel, sizes, has_out, layer), out...  141 us
    pallas_call x2, Pallas kernels, recurrence_call(): pl.pallas_call(functools.partial(recurrence_kernel, layer, heads, new), g...  22.7 us
    unnamed x1, blocking collectives  6.38 us
    unnamed x15, local copies, waits for them, and re-layouts  5.94 us
    dot_general x1, matrix products, local(): moved = jnp.dot(spread, xc, preferred_element_type=F32).astype(BF16)  4.25 us

profile of v1, /device:TPU:0, one launch (start us, length us, event | category | flops | bytes accessed | tf_op | source)
XLA Modules:
  0.0 185.1 jit_solution(10866366373370330894)
XLA Ops:
  0.6 1.2 dynamic-slice
  2.5 0.9 dynamic-update-slice
  3.4 6.4 %all-reduce = s32[128]{0:T(128)S(1)} all-reduce(s32[128]{0:T(128)S(1)} %dynamic-update-slice), channel_id=1, replica_groups=mesh['tp'=8,'dp'=4] {'dp'}, use_global_device_ids=true, to_apply=%add | all-reduce | flops 128 | bytes 1024
  9.8 0.1 select_reduce_fusion
  9.9 0.7 slice_bitcast_fusion
  10.6 0.7 fusion.1
  11.3 0.1 reshape.161
  11.4 0.1 add_select_fusion
  11.5 0.7 select_n.43.refs_0_
  12.2 0.1 select_n.42
  12.3 0.1 copy.30.ext_ref
  12.5 0.1 copy.28.ext_ref
  12.6 1.0 select_n.46.refs_2_.refs_4_
  13.6 0.0 copy-start.4
  13.6 0.0 copy-start.5
  13.6 26.6 %comm0.1 = (bf16[256,2048]{1,0:T(8,128)(2,1)}, bf16[384,1024]{1,0:T(8,128)(2,1)}) custom-call(s32[1,1024]{1,0:T(1,128)} %select_n.43.refs_0_, bf16[1024,1024]{1,0:T(8,128)(2,1)} %refs_1_.1, s32[1024,1]{1,0:T(8,128)} %select_n.46.refs_2_.refs_4_, f32[2,1024]{1,0:T(2,128)} %refs_5_.3, bf16[2,1024,512]{2,1,0:T(8,128)(2,1)} %refs_6_.3, ...), custom_call_target="tpu_custom_call" | custom-call | tf_op jit(solution)/shard_map/comm0/pallas_call | solution.py:351
  40.2 0.0 copy-done.4
  40.2 0.0 copy-done.5
  40.3 0.0 copy-start.1
  40.3 1.2 copy-done.1
  41.5 11.4 %recurrence0.1 = (bf16[256,512]{1,0:T(8,128)(2,1)S(1)}, f32[2,32,4,128,128]{4,3,2,1,0:T(8,128)}) custom-call(bf16[256,2048]{1,0:T(8,128)(2,1)S(1)} %copy-done.1, f32[256,5]{1,0:T(8,128)S(1)} %copy.28.ext_ref, f32[2,512]{1,0:T(2,128)S(1)} %copy-done.4, f32[2,512]{1,0:T(2,128)S(1)} %copy-done.5, f32[2,32,4,128,128]{4,3,2,1,0:T(8,128)} %s_ref.3), custom_call_target="tpu_custom_call" | custom-call | tf_op jit(solution)/shard_map/recurrence0/pallas_call | solution.py:448
  52.9 0.0 copy-start.2
  52.9 0.7 copy-done.2
  53.6 69.0 %comm1.1 = (bf16[256,2048]{1,0:T(8,128)(2,1)}, bf16[384,1024]{1,0:T(8,128)(2,1)}) custom-call(s32[1,1024]{1,0:T(1,128)} %select_n.43.refs_0_, bf16[256,512]{1,0:T(8,128)(2,1)} %copy-done.2, bf16[384,1024]{1,0:T(8,128)(2,1)} %get-tuple-element.12.refs_2_, bf16[2,512,1024]{2,1,0:T(8,128)(2,1)} %refs_3_.5, s32[1024,1]{1,0:T(8,128)} %select_n.46.refs_2_.refs_4_, ...), custom_call_target="tpu_custom_call" | custom-call | tf_op jit(solution)/shard_map/comm1/pallas_call | solution.py:351
  122.6 0.0 copy-start
  122.6 1.2 copy-done
  123.8 11.4 %recurrence1.1 = (bf16[256,512]{1,0:T(8,128)(2,1)S(1)}, f32[2,32,4,128,128]{4,3,2,1,0:T(8,128)}) custom-call(bf16[256,2048]{1,0:T(8,128)(2,1)S(1)} %copy-done, f32[256,5]{1,0:T(8,128)S(1)} %copy.30.ext_ref, f32[2,512]{1,0:T(2,128)S(1)} %copy-done.4, f32[2,512]{1,0:T(2,128)S(1)} %copy-done.5, ...), custom_call_target="tpu_custom_call", output_to_operand_aliasing={{1}: (5, {})} | custom-call | tf_op jit(solution)/shard_map/recurrence1/pallas_call | solution.py:448
  135.2 0.0 copy-start.3
  135.2 0.7 copy-done.3
  135.9 45.0 %comm2.1 = bf16[384,1024]{1,0:T(8,128)(2,1)} custom-call(s32[1,1024]{1,0:T(1,128)} %select_n.43.refs_0_, bf16[256,512]{1,0:T(8,128)(2,1)} %copy-done.3, bf16[384,1024]{1,0:T(8,128)(2,1)} %get-tuple-element.16.refs_2_, bf16[2,512,1024]{2,1,0:T(8,128)(2,1)} %refs_3_.5), custom_call_target="tpu_custom_call" | custom-call | tf_op jit(solution)/shard_map/comm2/pallas_call | solution.py:351
  180.9 4.2 %convert_select_fusion = bf16[1024,1024]{1,0:T(8,128)(2,1)} fusion(bf16[1024,1024]{1,0:T(8,128)(2,1)} %refs_1_.1, pred[1024]{0:T(1024)(128)(4,1)S(1)} %broadcast_compare_fusion, bf16[384,1024]{1,0:T(8,128)(2,1)} %comm2.1, s32[1024]{0:T(1024)S(1)} %select_n.42), kind=kOutput, calls=%fused_computation | convolution fusion | flops 807796736 | bytes 4985856 | tf_op jit(solution)/shard_map/dot_general | solution.py:520
  (3 shorter events, 0.0 us)
Async XLA Ops:
  13.6 26.6 %copy-start.4 = (f32[2,512]{1,0:T(2,128)S(1)}, f32[2,512]{1,0:T(2,128)}, u32[]{:S(2)}) copy-start(f32[2,512]{1,0:T(2,128)} %low_ref.3) | copy-start | bytes 12292
  13.6 26.6 %copy-start.5 = (f32[2,512]{1,0:T(2,128)S(1)}, f32[2,512]{1,0:T(2,128)}, u32[]{:S(2)}) copy-start(f32[2,512]{1,0:T(2,128)} %gain_ref.3) | copy-start | bytes 12292
  40.3 1.2 copy-start.1
  52.9 0.7 copy-start.2
  122.6 1.2 copy-start
  135.2 0.7 copy-start.3
